TPU v7x, 128 devices: a whole 4x4x4 slice. The times are simulated.
128 devices in a mesh: sp: 64 (over z, y, x), tp: 2 (over core).
Axes of the slice: x: 4, y: 4, z: 4, core: 2. Of those that a mesh axis runs over, the one named last changes fastest.
Arguments:
- queries: bfloat16 [8192, 1024], P('sp', 'tp'), may hold values from -6 to 6
- keys: bfloat16 [8192, 1024], P('sp', 'tp'), may hold values from -6 to 6
- values: bfloat16 [8192, 2048], P('sp', 'tp'), may hold values from -6 to 6
- out_gate: bfloat16 [8192, 2048], P('sp', 'tp'), may hold values from -6 to 6
- decay_rate: float32 [8], P('tp'), may hold values from 0 to 1
- residual: bfloat16 [8192, 2048], P(('sp', 'tp')), may hold values from -6 to 6
- out_weight: bfloat16 [2048, 2048], P('tp'), may hold values from -0.125 to 0.125
- ffn_gain: float32 [2048], replicated, may hold values from 0.1 to 1.9
- route_ids: int32 [8192, 4], P(('sp', 'tp')), may hold values from 0 to 63, all different within a row; in each aligned block of 64 rows (0 to 63, 64 to 127, ...) at most 8 rows name the same one
- route_weights: float32 [8192, 4], P(('sp', 'tp')), may hold values from 0.1 to 1
- gate_up: bfloat16 [64, 2048, 2048], P('sp', None, 'tp'), may hold values from -0.375 to 0.375
- lin_up: bfloat16 [64, 2048, 2048], P('sp', None, 'tp'), may hold values from -0.375 to 0.375
- down_weight: bfloat16 [64, 2048, 2048], P('sp', 'tp'), may hold values from -0.03125 to 0.03125
Outputs:
- layer_out: bfloat16 [8192, 2048], P(('sp', 'tp'))
Inputs may be any that keep to these rules, and one draw needn't show every extreme that they name: `route_ids`: within the rows of one device (aligned blocks of 64 rows), no expert is named by more than 8 entries, a bound that some block reaches; the 4 experts of a row differ.
All inputs are finite; a program needn't handle non-finite values.
Results may differ from a plain program's by a relative error of at most 0.03.
Values may be sent and summed in bfloat16 or wider, within the bound.
A program may use at most 128 MiB of HBM per device.

v0:
```python
import jax
import jax.numpy as jnp
from jax import lax
from jax.sharding import Mesh
from jax.sharding import PartitionSpec as P

D = 2048
DK = 128
DV = 256
SP = ("sp_0", "sp_1", "sp_2")
SP_TP = ("sp_0", "sp_1", "sp_2", "tp")


EPS = 1e-05
CLAMP_LIMIT = 7.0
SIGMOID_SLOPE = 1.702
TOP_PRECISION = lax.Precision.HIGHEST


def filled_with(array, identity):
    return jax.tree.map(
        lambda a, e: jnp.broadcast_to(jnp.asarray(e, a.dtype), a.shape), array, identity
    )


def entering(array, axes, combine, identity):
    before = start = filled_with(array, identity)
    total = array
    for axis in reversed(axes):
        peers, mine = (lax.axis_size(axis), lax.axis_index(axis))
        pieces = jax.tree.map(
            lambda part, kind: lax.all_gather(part.astype(kind), axis),
            total,
            (jnp.bfloat16, jnp.bfloat16),
        )
        inside, total = (start, start)
        for k in range(peers):
            passed = k < mine
            total = combine(
                total, jax.tree.map(lambda part, own: part[k].astype(own.dtype), pieces, array)
            )
            inside = jax.tree.map(lambda new, old: jnp.where(passed, new, old), total, inside)
        before = combine(inside, before)
    return before


def in_blocks(array, dim, peers):
    before, after = (array.shape[:dim], array.shape[dim + 1 :])
    return jnp.moveaxis(array.reshape(*before, peers, -1, *after), dim, 0)


def summed_on_arrival(array, axis, dim):
    tiles = in_blocks(array, dim, lax.axis_size(axis))
    arrived = lax.all_to_all(tiles, axis, split_axis=0, concat_axis=0, tiled=True)
    return arrived.astype(jnp.float32).sum(axis=0)


def expert_act(row_block, gate_part, lin_part):
    gate_pre = jnp.dot(row_block, gate_part, preferred_element_type=jnp.float32)
    lin_pre = jnp.dot(row_block, lin_part, preferred_element_type=jnp.float32)
    gate_clip = jnp.minimum(gate_pre, CLAMP_LIMIT)
    lin_clip = jnp.clip(lin_pre, -CLAMP_LIMIT, CLAMP_LIMIT)
    return (gate_clip * jax.nn.sigmoid(SIGMOID_SLOPE * gate_clip) * (lin_clip + 1.0)).astype(
        jnp.bfloat16
    )


def combine_state(before_part, after_part):
    return (
        before_part[0] * after_part[0],
        after_part[0][:, None, None] * before_part[1] + after_part[1],
    )


def local(
    queries,
    keys,
    values,
    out_gate,
    decay_rate,
    residual,
    out_weight,
    ffn_gain,
    route_ids,
    route_weights,
    gate_up,
    lin_up,
    down_weight,
):
    block_len = queries.shape[0]
    local_heads = decay_rate.shape[0]
    log_gamma = -decay_rate
    query_heads = queries.astype(jnp.float32).reshape(block_len, local_heads, DK).transpose(1, 0, 2)
    per_head_keys = keys.astype(jnp.float32).reshape(block_len, local_heads, DK).transpose(
        1, 0, 2
    ) * DK ** (-0.5)
    per_head_values = (
        values.astype(jnp.float32).reshape(block_len, local_heads, DV).transpose(1, 0, 2)
    )
    positions = jnp.arange(block_len, dtype=jnp.float32)
    offsets = positions[:, None] - positions[None, :]
    causal = offsets >= 0
    decay_mask = jnp.where(
        causal[None], jnp.exp(jnp.where(causal, offsets, 0.0)[None] * log_gamma[:, None, None]), 0.0
    )
    trailing_decay = jnp.exp((block_len - 1.0 - positions)[None, :] * log_gamma[:, None])
    lead_decay = jnp.exp((positions + 1.0)[None, :] * log_gamma[:, None])
    chain_decay = jnp.exp(block_len * log_gamma)
    attention_scores = (
        jnp.einsum("hqd,hkd->hqk", query_heads, per_head_keys, precision=TOP_PRECISION) * decay_mask
    )
    intra_block_term = jnp.einsum(
        "zfp,zpn->zfn", attention_scores, per_head_values, precision=TOP_PRECISION
    )
    state_delta = jnp.einsum(
        "mxs,mxq->msq",
        per_head_keys * trailing_decay[:, :, None],
        per_head_values,
        precision=TOP_PRECISION,
    )
    identity = (jnp.ones_like(chain_decay), jnp.zeros_like(state_delta))
    carried = entering((chain_decay, state_delta), SP, combine_state, identity)[1]
    cross_term = (
        jnp.einsum("hqd,hdv->hqv", query_heads, carried, precision=TOP_PRECISION)
        * lead_decay[:, :, None]
    )
    retained = intra_block_term + cross_term
    normed = retained * lax.rsqrt(jnp.mean(retained * retained, axis=-1, keepdims=True) + EPS)
    gated = (
        normed.transpose(1, 0, 2).reshape(block_len, local_heads * DV)
        * jax.nn.silu(out_gate.astype(jnp.float32))
    ).astype(jnp.bfloat16)
    mix_rows = summed_on_arrival(
        jnp.dot(gated, out_weight, preferred_element_type=jnp.float32).astype(jnp.bfloat16), "tp", 0
    )
    mixed = (residual.astype(jnp.float32) + mix_rows).astype(jnp.bfloat16)
    mixed_wide = mixed.astype(jnp.float32)
    normed_rows = (
        mixed_wide
        * lax.rsqrt(jnp.mean(mixed_wide * mixed_wide, axis=-1, keepdims=True) + EPS)
        * ffn_gain
    ).astype(jnp.bfloat16)
    experts = lax.axis_size(SP)
    own_rows = route_ids.shape[0]
    top_count = route_ids.shape[1]
    capacity = own_rows * top_count * lax.axis_size("tp") // experts
    flat_ids = route_ids.reshape(-1)
    one_hot = (flat_ids[:, None] == jnp.arange(experts, dtype=jnp.int32)[None, :]).astype(jnp.int32)
    slot_rank = jnp.sum(one_hot * (jnp.cumsum(one_hot, axis=0) - 1), axis=1)
    slot_index = flat_ids * capacity + slot_rank
    source_row = jnp.arange(own_rows * top_count, dtype=jnp.int32) // top_count
    slot_source = (
        jnp.full((experts * capacity,), own_rows, jnp.int32).at[slot_index].set(source_row)
    )
    padded = jnp.concatenate([normed_rows, jnp.zeros((1, D), jnp.bfloat16)], axis=0)
    outgoing = padded[slot_source].reshape(experts, capacity, D)
    gate_half = gate_up[0]
    lin_half = lin_up[0]
    down_half = down_weight[0]
    pair_rows = lax.all_gather(
        lax.all_to_all(outgoing, SP, split_axis=0, concat_axis=0, tiled=True),
        "tp",
        axis=0,
        tiled=True,
    )
    activation = expert_act(pair_rows.reshape(-1, D), gate_half, lin_half)
    partial_value = jnp.dot(activation, down_half, preferred_element_type=jnp.float32).reshape(
        pair_rows.shape
    )
    summed = summed_on_arrival(partial_value.astype(jnp.bfloat16), "tp", 0)
    returned = lax.all_to_all(
        summed.astype(jnp.bfloat16), SP, split_axis=0, concat_axis=0, tiled=True
    )
    picked = (
        returned.reshape(experts * capacity, D)[slot_index]
        .reshape(own_rows, top_count, D)
        .astype(jnp.float32)
    )
    expert_sum = jnp.sum(picked * route_weights[:, :, None], axis=1)
    return (mixed_wide + expert_sum).astype(jnp.bfloat16)


def solution(mesh):
    torus = Mesh(mesh.devices.reshape(4, 4, 4, mesh.shape["tp"]), ("sp_0", "sp_1", "sp_2", "tp"))
    in_specs = (
        P(SP, "tp"),
        P(SP, "tp"),
        P(SP, "tp"),
        P(SP, "tp"),
        P("tp"),
        P(SP_TP, None),
        P("tp", None),
        P(),
        P(SP_TP, None),
        P(SP_TP, None),
        P(SP, None, "tp"),
        P(SP, None, "tp"),
        P(SP, "tp", None),
    )
    out_specs = P(SP_TP, None)
    return jax.shard_map(local, mesh=torus, in_specs=in_specs, out_specs=out_specs, check_vma=False)
```

profile of v0, /device:TPU:1, one launch (start us, length us, event | category | flops | bytes accessed | tf_op | source)
XLA Modules:
  0.0 243.3 jit_solution(16506866070765259608)
XLA Ops:
  7.3 1.0 copy.78
  8.3 2.0 convolution_convert_fusion.1
  10.5 1.3 dynamic-slice
  12.7 9.3 %all-reduce.1 = bf16[16]{0:T(256)(128)(2,1)S(1)} all-reduce(bf16[16]{0:T(256)(128)(2,1)S(1)} %dynamic-update-slice), channel_id=2, replica_groups=mesh['sp_0'=4,'sp_1'=4,'sp_2'=4,'tp'=2] {'sp_2'}, use_global_device_ids=true, to_apply=%add.1 | all-reduce | flops 16 | bytes 64
  22.1 8.3 %all-gather.2 = bf16[4,1,4]{2,1,0:T(2,128)(2,1)S(1)} all-gather(bf16[1,1,4]{2,1,0:T(2,128)(2,1)S(1)} %get-tuple-element.9), channel_id=1, replica_groups=mesh['sp_0'=4,'sp_1'=4,'sp_2'=4,'tp'=2] {'sp_1'}, dimensions={0}, use_global_device_ids=true | all-gather | bytes 40 | tf_op jit(solution)/shard_map/all_gather | solution.py:32
  30.6 5.2 %all-gather.15.cloned.1.call-done = bf16[16,128,256]{2,1,0:T(8,128)(2,1)} async-done(((bf16[4,128,256]{2,1,0:T(8,128)(2,1)}), bf16[16,128,256]{2,1,0:T(8,128)(2,1)}) %all-gather.15.cloned.1.call-update) | async-done | bytes 1048592 | tf_op jit(solution)/shard_map/all_gather | solution.py:32
  35.7 2.2 fusion.60
  38.0 7.9 %all-gather.3 = bf16[4,1,4]{2,1,0:T(2,128)(2,1)S(1)} all-gather(bf16[1,1,4]{2,1,0:T(2,128)(2,1)S(1)} %fusion.142), channel_id=1, replica_groups=mesh['sp_0'=4,'sp_1'=4,'sp_2'=4,'tp'=2] {'sp_0'}, dimensions={0}, use_global_device_ids=true | all-gather | bytes 40 | tf_op jit(solution)/shard_map/all_gather | solution.py:32
  45.9 0.8 copy.66
  46.9 1.1 copy.64
  49.9 12.7 %all-gather.9.cloned.1.call-done = bf16[4,4,128,256]{3,2,1,0:T(8,128)(2,1)} async-done(((bf16[1,4,128,256]{3,2,1,0:T(8,128)(2,1)}), bf16[4,4,128,256]{3,2,1,0:T(8,128)(2,1)}) %all-gather.9.cloned.1.call-update) | async-done | bytes 1048592 | tf_op jit(solution)/shard_map/all_gather | solution.py:32
  62.6 2.2 fusion.46
  64.8 1.4 scatter_custom_fusion
  66.9 22.7 %all-gather.11.cloned.1.call-done = bf16[4,4,128,256]{3,2,1,0:T(8,128)(2,1)} async-done(((bf16[1,4,128,256]{3,2,1,0:T(8,128)(2,1)}), bf16[4,4,128,256]{3,2,1,0:T(8,128)(2,1)}) %all-gather.11.cloned.1.call-update) | async-done | bytes 1048592 | tf_op jit(solution)/shard_map/all_gather | solution.py:32
  89.6 3.1 %fusion.29 = f32[4,256,128]{1,2,0:T(8,128)S(1)} fusion(bf16[4,4,128,256]{3,2,1,0:T(8,128)(2,1)} %all-gather.11.cloned.1.call-done, f32[4]{0:T(128)S(1)} %get-tuple-element.20, f32[4]{0:T(128)S(1)} %get-tuple-element.24, f32[4]{0:T(128)S(1)} %get-tuple-element.25, f32[4]{0:T(128)S(1)} %get-tuple-element.23, f32[4]{0:T(128)S(1)} %get-tuple-element.14, ...), kind=kOutput, calls=%fused_computation.49 | convolution fusion | flops 207749120 | bytes 3801324 | tf_op jit(solution)/shard_map/hqd,hdv->hqv/dot_general | solution.py:124
  93.9 2.9 %convolution_convert_fusion = bf16[128,2048]{1,0:T(8,128)(2,1)S(1)} fusion(bf16[128,1024]{0,1:T(8,128)(2,1)S(1)} %fusion.83, bf16[1024,2048]{1,0:T(8,128)(2,1)} %param.19), kind=kOutput, calls=%fused_computation.13 | convolution fusion | flops 537133056 | bytes 4980736 | tf_op jit(solution)/shard_map/dot_general | solution.py:134
  96.8 6.5 %all_to_all.20 = bf16[2,64,2048]{2,1,0:T(8,128)(2,1)S(1)} all-to-all(bf16[2,64,2048]{2,1,0:T(8,128)(2,1)S(1)} %bitcast.272), channel_id=1, replica_groups=mesh['sp_0'=4,'sp_1'=4,'sp_2'=4,'tp'=2] {'tp'}, dimensions={0} | all-to-all | bytes 1048576 | tf_op jit(solution)/shard_map/all_to_all | solution.py:54
  103.8 2.5 %gather_fusion = bf16[512,2048]{1,0:T(8,128)(2,1)S(1)} fusion(bf16[65,2048]{1,0:T(8,128)(2,1)S(1)} %concatenate.3, s32[1024]{0:T(1024)S(1)} %pad_clamp_fusion.1), kind=kCustom, calls=%fused_computation | custom fusion | bytes 4196352 | tf_op jit(solution)/shard_map/gather | solution.py:156
  106.3 37.8 %all_to_all.21 = bf16[64,8,2048]{2,1,0:T(8,128)(2,1)} all-to-all(bf16[64,8,2048]{2,1,0:T(8,128)(2,1)S(1)} %bitcast.268), channel_id=1, replica_groups=mesh['sp_0'=4,'sp_1'=4,'sp_2'=4,'tp'=2] {'sp_0','sp_1','sp_2'}, dimensions={0} | all-to-all | bytes 4194304 | tf_op jit(solution)/shard_map/all_to_all | solution.py:161
  144.2 15.0 %all-gather.13.cloned.1.call-done = bf16[128,8,2048]{2,1,0:T(8,128)(2,1)} async-done(((bf16[64,8,2048]{2,1,0:T(8,128)(2,1)}), bf16[128,8,2048]{2,1,0:T(8,128)(2,1)}) %all-gather.13.cloned.1.call-update) | async-done | bytes 4194320 | tf_op jit(solution)/shard_map/all_gather | solution.py:160
  159.2 7.6 %fusion.2 = f32[1024,1024]{1,0:T(8,128)S(1)} fusion(bf16[1,2048,1024]{2,1,0:T(8,128)(2,1)} %param.24, bf16[128,8,2048]{2,1,0:T(8,128)(2,1)} %all-gather.13.cloned.1.call-done), kind=kOutput, calls=%fused_computation.5 | convolution fusion | flops 4294967296 | bytes 12582912 | tf_op jit(solution)/shard_map/dot_general | solution.py:60
  166.9 5.8 %fusion.16 = bf16[128,8,1024]{2,1,0:T(8,128)(2,1)S(1)} fusion(f32[1024,1024]{1,0:T(8,128)S(1)} %fusion.2, bf16[1,2048,1024]{2,1,0:T(8,128)(2,1)S(1)} %copy-done.5, bf16[128,8,2048]{2,1,0:T(8,128)(2,1)S(1)} %copy-done.7), kind=kOutput, calls=%fused_computation.16 | convolution fusion | flops 4305453056 | bytes 14680064 | tf_op jit(solution)/shard_map/dot_general | solution.py:59
  172.6 5.2 %fusion.8 = bf16[128,8,2048]{2,0,1:T(8,128)(2,1)S(1)} fusion(bf16[1,1024,2048]{2,1,0:T(8,128)(2,1)S(1)} %copy-done.6, bf16[128,8,1024]{2,1,0:T(8,128)(2,1)S(1)} %fusion.16), kind=kOutput, calls=%fused_computation.12 | convolution fusion | flops 4297064448 | bytes 10485760 | tf_op jit(solution)/shard_map/dot_general | solution.py:167
  178.4 8.0 %all_to_all.22 = bf16[2,64,8,2048]{3,1,2,0:T(8,128)(2,1)} all-to-all(bf16[2,64,8,2048]{3,1,2,0:T(8,128)(2,1)S(1)} %copy.70), channel_id=1, replica_groups=mesh['sp_0'=4,'sp_1'=4,'sp_2'=4,'tp'=2] {'tp'}, dimensions={0} | all-to-all | bytes 8388608 | tf_op jit(solution)/shard_map/all_to_all | solution.py:54
  186.4 3.5 %reduce_sum.64 = bf16[64,8,2048]{2,0,1:T(8,128)(2,1)S(1)} reduce(bf16[2,64,8,2048]{3,1,2,0:T(8,128)(2,1)} %all_to_all.22, bf16[]{:T(256)} %constant.77.clone.1), dimensions={0}, to_apply=%region_7.8 | reduce | flops 1048576 | bytes 6291458 | tf_op jit(solution)/shard_map/reduce_sum | solution.py:55
  189.9 2.5 %copy.72 = bf16[64,8,2048]{2,1,0:T(8,128)(2,1)} copy(bf16[64,8,2048]{2,0,1:T(8,128)(2,1)S(1)} %reduce_sum.64) | data formatting | bytes 4194304 | tf_op jit(solution)/shard_map/reduce_sum | solution.py:55
  192.4 10.3 %all-to-all-start.3 = ((bf16[64,8,2048]{2,1,0:T(8,128)(2,1)}), bf16[64,8,2048]{2,1,0:T(8,128)(2,1)S(1)}, u32[]{:S(2)}, u32[]{:S(2)}) async-start(bf16[64,8,2048]{2,1,0:T(8,128)(2,1)} %copy.72), calls=%async_computation.3 | async-start | bytes 4194304 | tf_op jit(solution)/shard_map/all_to_all | solution.py:171
  202.8 0.7 copy.73
  203.5 28.0 %all-to-all-done.3 = bf16[64,8,2048]{2,1,0:T(8,128)(2,1)S(1)} async-done(((bf16[64,8,2048]{2,1,0:T(8,128)(2,1)}), bf16[64,8,2048]{2,1,0:T(8,128)(2,1)S(1)}, u32[]{:S(2)}, u32[]{:S(2)}) %all-to-all-start.3) | async-done | bytes 2097184 | tf_op jit(solution)/shard_map/all_to_all | solution.py:171
  231.5 1.4 gather_fusion.1
  233.6 2.4 multiply_reduce_fusion
  236.0 0.8 fusion.64
  (69 shorter events, 6.9 us)
Async XLA Ops:
  6.5 59.9 %copy-start = (bf16[128,512]{1,0:T(8,128)(2,1)S(1)}, bf16[128,512]{1,0:T(8,128)(2,1)}, u32[]{:S(2)}) copy-start(bf16[128,512]{1,0:T(8,128)(2,1)} %param.13) | copy-start | bytes 393220
  6.5 29.2 %all-gather.15.cloned.1.call-start = ((), (), s32[]{:S(2)}) async-start(), calls=%async_computation.7 | async-start | bytes 1310720 | tf_op jit(solution)/shard_map/all_gather | solution.py:32
  10.4 52.2 %all-gather.9.cloned.1.call-start = ((), (), s32[]{:S(2)}) async-start(), calls=%async_computation.4 | async-start | bytes 1310720 | tf_op jit(solution)/shard_map/all_gather | solution.py:32
  37.9 51.6 %all-gather.11.cloned.1.call-start = ((), (), s32[]{:S(2)}) async-start(), calls=%async_computation.5 | async-start | bytes 1310720 | tf_op jit(solution)/shard_map/all_gather | solution.py:32
  64.8 94.4 %all-gather.13.cloned.1.call-start = ((), (), s32[]{:S(2)}) async-start(), calls=%async_computation.6 | async-start | bytes 6291456 | tf_op jit(solution)/shard_map/all_gather | solution.py:160
  66.8 25.9 %copy-start.1 = (bf16[128,1024]{1,0:T(8,128)(2,1)S(1)}, bf16[128,1024]{1,0:T(8,128)(2,1)}, u32[]{:S(2)}) copy-start(bf16[128,1024]{1,0:T(8,128)(2,1)} %param.15) | copy-start | bytes 786436
  93.7 9.7 %copy-start.2 = (bf16[64,2048]{1,0:T(8,128)(2,1)S(1)}, bf16[64,2048]{1,0:T(8,128)(2,1)}, u32[]{:S(2)}) copy-start(bf16[64,2048]{1,0:T(8,128)(2,1)} %param.18) | copy-start | bytes 786436
  93.9 9.8 %copy-start.3 = (f32[2048]{0:T(1024)S(1)}, f32[2048]{0:T(1024)}, u32[]{:S(2)}) copy-start(f32[2048]{0:T(1024)} %param.20) | copy-start | bytes 24580
  159.2 7.7 %copy-start.5 = (bf16[1,2048,1024]{2,1,0:T(8,128)(2,1)S(1)}, bf16[1,2048,1024]{2,1,0:T(8,128)(2,1)}, u32[]{:S(2)}) copy-start(bf16[1,2048,1024]{2,1,0:T(8,128)(2,1)} %param.23) | copy-start | bytes 12582916
  159.2 7.7 %copy-start.7 = (bf16[128,8,2048]{2,1,0:T(8,128)(2,1)S(1)}, bf16[128,8,2048]{2,1,0:T(8,128)(2,1)}, u32[]{:S(2)}) copy-start(bf16[128,8,2048]{2,1,0:T(8,128)(2,1)} %all-gather.13.cloned.1.call-done) | copy-start | bytes 12582916
  166.8 5.8 %copy-start.6 = (bf16[1,1024,2048]{2,1,0:T(8,128)(2,1)S(1)}, bf16[1,1024,2048]{2,1,0:T(8,128)(2,1)}, u32[]{:S(2)}) copy-start(bf16[1,1024,2048]{2,1,0:T(8,128)(2,1)} %param.25) | copy-start | bytes 12582916
  189.9 12.9 %copy-start.4 = (f32[64,4]{0,1:T(4,128)S(1)}, f32[64,4]{0,1:T(4,128)}, u32[]{:S(2)}) copy-start(f32[64,4]{0,1:T(4,128)} %param.22) | copy-start | bytes 3076
  192.4 39.1 %all-to-all-start.3 = ((bf16[64,8,2048]{2,1,0:T(8,128)(2,1)}), bf16[64,8,2048]{2,1,0:T(8,128)(2,1)S(1)}, u32[]{:S(2)}, u32[]{:S(2)}) async-start(bf16[64,8,2048]{2,1,0:T(8,128)(2,1)} %copy.72), calls=%async_computation.3 | async-start | bytes 4194304 | tf_op jit(solution)/shard_map/all_to_all | solution.py:171
Sparse Core Ops, SparseCore 0:
  10.5 25.1 all-gather.14
  38.1 24.4 all-gather.8
  64.9 24.6 all-gather.10
  144.3 14.8 all-gather.12
where the time goes:
time: 245 us; the launch traced here: 243 us
  waiting for transfers between devices  83.7 us (34%)
  blocking collectives  77.9 us (32%)
  matrix products  27.6 us (11%)
  local copies, waits for them, and re-layouts  15 us (6%)
  other arithmetic  14.4 us (6%)
  between operations  14.2 us (6%)
  starting transfers between devices  10.5 us (4%)
    all_gather x3, waiting for transfers between devices, entering(): lax.all_gather(part.astype(kind), axis)  40.6 us
    all_to_all x1, blocking collectives, local(): lax.all_to_all(outgoing, SP, split_axis=0, concat_axis=0, tiled=True)  37.8 us
    all_to_all x1, waiting for transfers between devices, local(): lax.all_to_all(summed.astype(jnp.bfloat16), SP, split_axis=0, concat_axis...  28 us
    all_gather x2, blocking collectives, entering(): lax.all_gather(part.astype(kind), axis)  16.2 us
    all_gather x1, waiting for transfers between devices, local(): lax.all_gather(lax.all_to_all(outgoing, SP, split_axis=0, concat_axis=0,...  15 us
    all_to_all x2, blocking collectives, summed_on_arrival(): lax.all_to_all(tiles, axis, split_axis=0, concat_axis=0, tiled=True)  14.6 us
    all_to_all x1, starting transfers between devices, local(): lax.all_to_all(summed.astype(jnp.bfloat16), SP, split_axis=0, concat_axis...  10.3 us
    unnamed x1, blocking collectives  9.26 us
  transfers between devices with their start and end apart: 5, of which 5 were waited for; matrix products, arithmetic and copies ran while one was open for 3% of the time, Pallas kernels for 0%

commit v1 on v0

--- a/solution.py
+++ b/solution.py
@@ -17,31 +17,20 @@
 TOP_PRECISION = lax.Precision.HIGHEST
 
 
-def filled_with(array, identity):
-    return jax.tree.map(
-        lambda a, e: jnp.broadcast_to(jnp.asarray(e, a.dtype), a.shape), array, identity
+def carried_state(state_delta, log_gamma, block_len):
+    peers, mine = (lax.axis_size(SP), lax.axis_index(SP))
+    heads = state_delta.shape[0]
+    pieces = state_delta.astype(jnp.bfloat16).reshape(peers, -1)
+    arrived = lax.all_to_all(pieces, SP, split_axis=0, concat_axis=0, tiled=True)
+    own_log = lax.dynamic_index_in_dim(log_gamma, mine * heads // peers, keepdims=False)
+    order = jnp.arange(peers, dtype=jnp.float32)
+    gap = order[:, None] - 1.0 - order[None, :]
+    weight = jnp.where(gap >= 0, jnp.exp(jnp.maximum(gap, 0.0) * block_len * own_log), 0.0)
+    before = jnp.dot(weight, arrived.astype(jnp.float32), precision=TOP_PRECISION)
+    returned = lax.all_to_all(
+        before.astype(jnp.bfloat16), SP, split_axis=0, concat_axis=0, tiled=True
     )
-
-
-def entering(array, axes, combine, identity):
-    before = start = filled_with(array, identity)
-    total = array
-    for axis in reversed(axes):
-        peers, mine = (lax.axis_size(axis), lax.axis_index(axis))
-        pieces = jax.tree.map(
-            lambda part, kind: lax.all_gather(part.astype(kind), axis),
-            total,
-            (jnp.bfloat16, jnp.bfloat16),
-        )
-        inside, total = (start, start)
-        for k in range(peers):
-            passed = k < mine
-            total = combine(
-                total, jax.tree.map(lambda part, own: part[k].astype(own.dtype), pieces, array)
-            )
-            inside = jax.tree.map(lambda new, old: jnp.where(passed, new, old), total, inside)
-        before = combine(inside, before)
-    return before
+    return returned.reshape(state_delta.shape).astype(jnp.float32)
 
 
 def in_blocks(array, dim, peers):
@@ -62,13 +51,6 @@
     lin_clip = jnp.clip(lin_pre, -CLAMP_LIMIT, CLAMP_LIMIT)
     return (gate_clip * jax.nn.sigmoid(SIGMOID_SLOPE * gate_clip) * (lin_clip + 1.0)).astype(
         jnp.bfloat16
-    )
-
-
-def combine_state(before_part, after_part):
-    return (
-        before_part[0] * after_part[0],
-        after_part[0][:, None, None] * before_part[1] + after_part[1],
     )
 
 
@@ -105,7 +87,6 @@
     )
     trailing_decay = jnp.exp((block_len - 1.0 - positions)[None, :] * log_gamma[:, None])
     lead_decay = jnp.exp((positions + 1.0)[None, :] * log_gamma[:, None])
-    chain_decay = jnp.exp(block_len * log_gamma)
     attention_scores = (
         jnp.einsum("hqd,hkd->hqk", query_heads, per_head_keys, precision=TOP_PRECISION) * decay_mask
     )
@@ -118,8 +99,7 @@
         per_head_values,
         precision=TOP_PRECISION,
     )
-    identity = (jnp.ones_like(chain_decay), jnp.zeros_like(state_delta))
-    carried = entering((chain_decay, state_delta), SP, combine_state, identity)[1]
+    carried = carried_state(state_delta, log_gamma, block_len)
     cross_term = (
         jnp.einsum("hqd,hdv->hqv", query_heads, carried, precision=TOP_PRECISION)
         * lead_decay[:, :, None]

time: 245 us -> 203 us (0.83)
  blocking collectives: 77.9 us -> 48.1 us
  waiting for transfers between devices: 83.7 us -> 55.6 us
  starting transfers between devices: 10.5 us -> 28.4 us
  matrix products: 27.6 us -> 24.4 us
    all_gather x3 -> x0, waiting for transfers between devices: 40.6 us -> none  [entering(): lax.all_gather(part.astype(kind), axis)]
    all_to_all x0 -> x2, starting transfers between devices: none -> 18 us  [the longest x1 12.1 us: carried_state(): lax.all_to_all(pieces, SP, split_axis=0, concat_axis=0, tiled=True)]
    all_gather x2 -> x0, blocking collectives: 16.2 us -> none  [entering(): lax.all_gather(part.astype(kind), axis)]
    all_to_all x0 -> x2, waiting for transfers between devices: none -> 12.7 us  [the longest x1 8.8 us: carried_state(): lax.all_to_all(before.astype(jnp.bfloat16), SP, split_axis=0, concat_axis...]
    unnamed x1 -> x0, blocking collectives: 9.26 us -> none
    all_to_all x0 -> x3, other arithmetic: none -> 4.52 us  [the longest x2 2.33 us: carried_state(): lax.all_to_all(before.astype(jnp.bfloat16), SP, split_axis=0, concat_axis...]
    convert_element_type x5 -> x0, other arithmetic: 4.44 us -> none  [the longest x2 4.36 us: entering(): part.astype(kind)]
    all_to_all x1, blocking collectives: 37.8 us -> 33.6 us  [local(): lax.all_to_all(outgoing, SP, split_axis=0, concat_axis=0, tiled=True)]
  transfers between devices with their start and end apart: 5 -> 4, of which waited for: 5 -> 4; matrix products, arithmetic and copies ran while one was open for 3% -> 3% of each run, Pallas kernels for 0% -> 0%
where the time goes in v1:
time: 203 us; the launch traced here: 201 us
  waiting for transfers between devices  55.6 us (27%)
  blocking collectives  48.1 us (24%)
  starting transfers between devices  28.4 us (14%)
  matrix products  24.4 us (12%)
  local copies, waits for them, and re-layouts  16.2 us (8%)
  between operations  14.4 us (7%)
  other arithmetic  14.3 us (7%)
    all_to_all x1, blocking collectives, local(): lax.all_to_all(outgoing, SP, split_axis=0, concat_axis=0, tiled=True)  33.6 us
    all_to_all x1, waiting for transfers between devices, local(): lax.all_to_all(summed.astype(jnp.bfloat16), SP, split_axis=0, concat_axis...  28 us
    all_gather x1, waiting for transfers between devices, local(): lax.all_gather(lax.all_to_all(outgoing, SP, split_axis=0, concat_axis=0,...  14.9 us
    all_to_all x2, blocking collectives, summed_on_arrival(): lax.all_to_all(tiles, axis, split_axis=0, concat_axis=0, tiled=True)  14.5 us
    all_to_all x1, starting transfers between devices, carried_state(): lax.all_to_all(pieces, SP, split_axis=0, concat_axis=0, tiled=True)  12.1 us
    all_to_all x1, starting transfers between devices, local(): lax.all_to_all(summed.astype(jnp.bfloat16), SP, split_axis=0, concat_axis...  10.3 us
    all_to_all x1, waiting for transfers between devices, carried_state(): lax.all_to_all(before.astype(jnp.bfloat16), SP, split_axis=0, concat_axis...  8.8 us
    dot_general x1, matrix products, expert_act(): lin_pre = jnp.dot(row_block, lin_part, preferred_element_type=jnp.float32)  7.64 us
  transfers between devices with their start and end apart: 4, of which 4 were waited for; matrix products, arithmetic and copies ran while one was open for 3% of the time, Pallas kernels for 0%

profile of v1, /device:TPU:1, one launch (start us, length us, event | category | flops | bytes accessed | tf_op | source)
XLA Modules:
  0.0 201.4 jit_solution(13798051839371577354)
XLA Ops:
  6.5 0.7 neg.10
  7.3 1.0 copy.102
  8.3 1.3 convolution_convert_fusion.2
  10.4 2.2 %reduce.4 = bf16[64,2048]{1,0:T(8,128)(2,1)S(1)} reduce(bf16[64,1,2048]{2,1,0:T(2,128)(2,1)S(1)} %all_to_all.35, bf16[]{:T(256)} %broadcast.223), dimensions={1}, to_apply=%all_to_all.35.reduce_sub_computation | reduce | bytes 524290 | tf_op jit(solution)/shard_map/all_to_all | solution.py:24
  12.6 0.9 reshape.247
  13.5 12.1 %all-to-all-start = ((bf16[64,2,1024]{2,1,0:T(2,128)(2,1)}), bf16[64,2,1024]{2,1,0:T(2,128)(2,1)S(1)}, u32[]{:S(2)}, u32[]{:S(2)}) async-start(bf16[64,2,1024]{2,1,0:T(2,128)(2,1)} %reshape.247), calls=%async_computation | async-start | bytes 524288 | tf_op jit(solution)/shard_map/all_to_all | solution.py:24
  25.7 0.8 copy.90
  29.8 1.4 scatter_custom_fusion
  31.2 3.9 %all-to-all-done = bf16[64,2,1024]{2,1,0:T(2,128)(2,1)S(1)} async-done(((bf16[64,2,1024]{2,1,0:T(2,128)(2,1)}), bf16[64,2,1024]{2,1,0:T(2,128)(2,1)S(1)}, u32[]{:S(2)}, u32[]{:S(2)}) %all-to-all-start) | async-done | bytes 262176 | tf_op jit(solution)/shard_map/all_to_all | solution.py:24
  35.8 0.8 reduce.5
  36.6 0.9 reshape.249
  37.5 5.9 %all-to-all-start.1 = ((bf16[64,2,1024]{2,1,0:T(2,128)(2,1)}), bf16[64,2,1024]{2,1,0:T(2,128)(2,1)S(1)}, u32[]{:S(2)}, u32[]{:S(2)}) async-start(bf16[64,2,1024]{2,1,0:T(2,128)(2,1)} %reshape.249), calls=%async_computation.1 | async-start | bytes 524288 | tf_op jit(solution)/shard_map/all_to_all | solution.py:30
  44.1 8.8 %all-to-all-done.1 = bf16[64,2,1024]{2,1,0:T(2,128)(2,1)S(1)} async-done(((bf16[64,2,1024]{2,1,0:T(2,128)(2,1)}), bf16[64,2,1024]{2,1,0:T(2,128)(2,1)S(1)}, u32[]{:S(2)}, u32[]{:S(2)}) %all-to-all-start.1) | async-done | bytes 262176 | tf_op jit(solution)/shard_map/all_to_all | solution.py:30
  53.1 1.5 reduce.1
  56.1 2.9 %convolution_convert_fusion = bf16[128,2048]{1,0:T(8,128)(2,1)S(1)} fusion(bf16[128,1024]{0,1:T(8,128)(2,1)S(1)} %fusion.35, bf16[1024,2048]{1,0:T(8,128)(2,1)} %param.19), kind=kOutput, calls=%fused_computation.13 | convolution fusion | flops 537133056 | bytes 4980736 | tf_op jit(solution)/shard_map/dot_general | solution.py:114
  59.0 6.5 %all_to_all.42 = bf16[2,64,2048]{2,1,0:T(8,128)(2,1)S(1)} all-to-all(bf16[2,64,2048]{2,1,0:T(8,128)(2,1)S(1)} %bitcast.118), channel_id=1, replica_groups=mesh['sp_0'=4,'sp_1'=4,'sp_2'=4,'tp'=2] {'tp'}, dimensions={0} | all-to-all | bytes 1048576 | tf_op jit(solution)/shard_map/all_to_all | solution.py:43
  66.0 2.5 %gather_fusion = bf16[512,2048]{1,0:T(8,128)(2,1)S(1)} fusion(bf16[65,2048]{1,0:T(8,128)(2,1)S(1)} %concatenate.3, s32[1024]{0:T(1024)S(1)} %pad_clamp_fusion.1), kind=kCustom, calls=%fused_computation | custom fusion | bytes 4196352 | tf_op jit(solution)/shard_map/gather | solution.py:136
  68.5 33.6 %all_to_all.43 = bf16[64,8,2048]{2,1,0:T(8,128)(2,1)} all-to-all(bf16[64,8,2048]{2,1,0:T(8,128)(2,1)S(1)} %bitcast.114), channel_id=1, replica_groups=mesh['sp_0'=4,'sp_1'=4,'sp_2'=4,'tp'=2] {'sp_0','sp_1','sp_2'}, dimensions={0} | all-to-all | bytes 4194304 | tf_op jit(solution)/shard_map/all_to_all | solution.py:141
  102.1 14.9 %all-gather.2.cloned.1.call-done = bf16[128,8,2048]{2,1,0:T(8,128)(2,1)} async-done(((bf16[64,8,2048]{2,1,0:T(8,128)(2,1)}), bf16[128,8,2048]{2,1,0:T(8,128)(2,1)}) %all-gather.2.cloned.1.call-update) | async-done | bytes 4194320 | tf_op jit(solution)/shard_map/all_gather | solution.py:140
  117.0 7.6 %fusion.2 = f32[1024,1024]{1,0:T(8,128)S(1)} fusion(bf16[1,2048,1024]{2,1,0:T(8,128)(2,1)} %param.24, bf16[128,8,2048]{2,1,0:T(8,128)(2,1)} %all-gather.2.cloned.1.call-done), kind=kOutput, calls=%fused_computation.5 | convolution fusion | flops 4294967296 | bytes 12582912 | tf_op jit(solution)/shard_map/dot_general | solution.py:49
  124.7 5.8 %fusion.17 = bf16[128,8,1024]{2,1,0:T(8,128)(2,1)S(1)} fusion(f32[1024,1024]{1,0:T(8,128)S(1)} %fusion.2, bf16[1,2048,1024]{2,1,0:T(8,128)(2,1)S(1)} %copy-done.6, bf16[128,8,2048]{2,1,0:T(8,128)(2,1)S(1)} %copy-done.8), kind=kOutput, calls=%fused_computation.18 | convolution fusion | flops 4305453056 | bytes 14680064 | tf_op jit(solution)/shard_map/dot_general | solution.py:48
  130.5 5.2 %fusion.8 = bf16[128,8,2048]{2,0,1:T(8,128)(2,1)S(1)} fusion(bf16[1,1024,2048]{2,1,0:T(8,128)(2,1)S(1)} %copy-done.7, bf16[128,8,1024]{2,1,0:T(8,128)(2,1)S(1)} %fusion.17), kind=kOutput, calls=%fused_computation.12 | convolution fusion | flops 4297064448 | bytes 10485760 | tf_op jit(solution)/shard_map/dot_general | solution.py:147
  136.2 8.0 %all_to_all.44 = bf16[2,64,8,2048]{3,1,2,0:T(8,128)(2,1)} all-to-all(bf16[2,64,8,2048]{3,1,2,0:T(8,128)(2,1)S(1)} %copy.94), channel_id=1, replica_groups=mesh['sp_0'=4,'sp_1'=4,'sp_2'=4,'tp'=2] {'tp'}, dimensions={0} | all-to-all | bytes 8388608 | tf_op jit(solution)/shard_map/all_to_all | solution.py:43
  144.2 3.5 %reduce_sum.64 = bf16[64,8,2048]{2,0,1:T(8,128)(2,1)S(1)} reduce(bf16[2,64,8,2048]{3,1,2,0:T(8,128)(2,1)} %all_to_all.44, bf16[]{:T(256)} %constant.96.clone.1), dimensions={0}, to_apply=%region_7.8 | reduce | flops 1048576 | bytes 6291458 | tf_op jit(solution)/shard_map/reduce_sum | solution.py:44
  147.7 2.5 %copy.96 = bf16[64,8,2048]{2,1,0:T(8,128)(2,1)} copy(bf16[64,8,2048]{2,0,1:T(8,128)(2,1)S(1)} %reduce_sum.64) | data formatting | bytes 4194304 | tf_op jit(solution)/shard_map/reduce_sum | solution.py:44
  150.2 10.3 %all-to-all-start.5 = ((bf16[64,8,2048]{2,1,0:T(8,128)(2,1)}), bf16[64,8,2048]{2,1,0:T(8,128)(2,1)S(1)}, u32[]{:S(2)}, u32[]{:S(2)}) async-start(bf16[64,8,2048]{2,1,0:T(8,128)(2,1)} %copy.96), calls=%async_computation.5 | async-start | bytes 4194304 | tf_op jit(solution)/shard_map/all_to_all | solution.py:151
  160.6 0.7 copy.97
  161.3 28.0 %all-to-all-done.5 = bf16[64,8,2048]{2,1,0:T(8,128)(2,1)S(1)} async-done(((bf16[64,8,2048]{2,1,0:T(8,128)(2,1)}), bf16[64,8,2048]{2,1,0:T(8,128)(2,1)S(1)}, u32[]{:S(2)}, u32[]{:S(2)}) %all-to-all-start.5) | async-done | bytes 2097184 | tf_op jit(solution)/shard_map/all_to_all | solution.py:151
  189.3 1.4 gather_fusion.1
  190.7 0.7 reshape.215
  191.4 2.4 %multiply_reduce_fusion = f32[64,2048]{1,0:T(8,128)S(1)} fusion(f32[64,4,2048]{2,1,0:T(4,128)S(1)} %reshape.215, f32[64,4]{1,0:T(8,128)} %copy.97), kind=kLoop, calls=%fused_computation.17 | loop fusion | flops 917504 | bytes 2622464 | tf_op jit(solution)/shard_map/reduce_sum | solution.py:159
  193.8 0.8 fusion.30
  (63 shorter events, 7.6 us)
Async XLA Ops:
  6.5 37.1 %copy-start = (bf16[128,512]{1,0:T(8,128)(2,1)S(1)}, bf16[128,512]{1,0:T(8,128)(2,1)}, u32[]{:S(2)}) copy-start(bf16[128,512]{1,0:T(8,128)(2,1)} %param.13) | copy-start | bytes 393220
  6.5 36.9 %copy-start.2 = (bf16[128,1024]{1,0:T(8,128)(2,1)S(1)}, bf16[128,1024]{1,0:T(8,128)(2,1)}, u32[]{:S(2)}) copy-start(bf16[128,1024]{1,0:T(8,128)(2,1)} %param.16) | copy-start | bytes 786436
  13.5 41.5 %copy-start.1 = (bf16[128,1024]{1,0:T(8,128)(2,1)S(1)}, bf16[128,1024]{1,0:T(8,128)(2,1)}, u32[]{:S(2)}) copy-start(bf16[128,1024]{1,0:T(8,128)(2,1)} %param.15) | copy-start | bytes 786436
  13.5 21.6 %all-to-all-start = ((bf16[64,2,1024]{2,1,0:T(2,128)(2,1)}), bf16[64,2,1024]{2,1,0:T(2,128)(2,1)S(1)}, u32[]{:S(2)}, u32[]{:S(2)}) async-start(bf16[64,2,1024]{2,1,0:T(2,128)(2,1)} %reshape.247), calls=%async_computation | async-start | bytes 524288 | tf_op jit(solution)/shard_map/all_to_all | solution.py:24
  37.5 15.4 %all-to-all-start.1 = ((bf16[64,2,1024]{2,1,0:T(2,128)(2,1)}), bf16[64,2,1024]{2,1,0:T(2,128)(2,1)S(1)}, u32[]{:S(2)}, u32[]{:S(2)}) async-start(bf16[64,2,1024]{2,1,0:T(2,128)(2,1)} %reshape.249), calls=%async_computation.1 | async-start | bytes 524288 | tf_op jit(solution)/shard_map/all_to_all | solution.py:30
  43.4 73.6 %all-gather.2.cloned.1.call-start = ((), (), s32[]{:S(2)}) async-start(), calls=%async_computation.6 | async-start | bytes 6291456 | tf_op jit(solution)/shard_map/all_gather | solution.py:140
  55.9 9.7 %copy-start.3 = (bf16[64,2048]{1,0:T(8,128)(2,1)S(1)}, bf16[64,2048]{1,0:T(8,128)(2,1)}, u32[]{:S(2)}) copy-start(bf16[64,2048]{1,0:T(8,128)(2,1)} %param.18) | copy-start | bytes 786436
  56.1 9.8 %copy-start.4 = (f32[2048]{0:T(1024)S(1)}, f32[2048]{0:T(1024)}, u32[]{:S(2)}) copy-start(f32[2048]{0:T(1024)} %param.20) | copy-start | bytes 24580
  117.0 7.7 %copy-start.6 = (bf16[1,2048,1024]{2,1,0:T(8,128)(2,1)S(1)}, bf16[1,2048,1024]{2,1,0:T(8,128)(2,1)}, u32[]{:S(2)}) copy-start(bf16[1,2048,1024]{2,1,0:T(8,128)(2,1)} %param.23) | copy-start | bytes 12582916
  117.0 7.7 %copy-start.8 = (bf16[128,8,2048]{2,1,0:T(8,128)(2,1)S(1)}, bf16[128,8,2048]{2,1,0:T(8,128)(2,1)}, u32[]{:S(2)}) copy-start(bf16[128,8,2048]{2,1,0:T(8,128)(2,1)} %all-gather.2.cloned.1.call-done) | copy-start | bytes 12582916
  124.7 5.8 %copy-start.7 = (bf16[1,1024,2048]{2,1,0:T(8,128)(2,1)S(1)}, bf16[1,1024,2048]{2,1,0:T(8,128)(2,1)}, u32[]{:S(2)}) copy-start(bf16[1,1024,2048]{2,1,0:T(8,128)(2,1)} %param.25) | copy-start | bytes 12582916
  147.7 12.9 %copy-start.5 = (f32[64,4]{0,1:T(4,128)S(1)}, f32[64,4]{0,1:T(4,128)}, u32[]{:S(2)}) copy-start(f32[64,4]{0,1:T(4,128)} %param.22) | copy-start | bytes 3076
  150.2 39.1 %all-to-all-start.5 = ((bf16[64,8,2048]{2,1,0:T(8,128)(2,1)}), bf16[64,8,2048]{2,1,0:T(8,128)(2,1)S(1)}, u32[]{:S(2)}, u32[]{:S(2)}) async-start(bf16[64,8,2048]{2,1,0:T(8,128)(2,1)} %copy.96), calls=%async_computation.5 | async-start | bytes 4194304 | tf_op jit(solution)/shard_map/all_to_all | solution.py:151
Sparse Core Ops, SparseCore 0:
  102.2 14.7 all-gather.1
